TPU v7x, 512 devices: a 4x2x32 block of a 4x8x32 slice. The times are simulated.
512 devices in a mesh: grp: 2 (over y), kv: 64 (over z, core), tp: 4 (over x).
Axes of the slice: x: 4, y: 2, z: 32, core: 2. Of those that a mesh axis runs over, the one named last changes fastest.
The devices are a block of a 4x8x32 slice.
Arguments:
- tokens: bfloat16 [65536, 2048], P(('grp', 'kv')), parts along dimension 0, may hold values from -72 to 72
- w_query: bfloat16 [2048, 1024], P(None, 'tp'), may hold values from -0.125 to 0.125
- w_key: bfloat16 [2048, 256], P(None, 'tp'), may hold values from -0.125 to 0.125
- w_value: bfloat16 [2048, 256], P(None, 'tp'), may hold values from -0.125 to 0.125
- w_out: bfloat16 [1024, 2048], P('tp'), may hold values from -0.1875 to 0.1875
- selection: int32 [4, 1024, 32], P('tp', ('grp', 'kv')), parts along dimension 1, may hold values from -1 to 511, as said below
Outputs:
- attended_out: bfloat16 [65536, 2048], P(('grp', 'kv', 'tp')), parts along dimension 0
There are 2 independent parts, one for each index of `grp`. A program takes and returns all parts, laid end to end along the dimension named above; an argument that names none is the same for every part. Nothing has to cross between parts.
Inputs may be any that keep to these rules, and one draw needn't show every extreme that they name: `selection`: entry 0 is the query block's own index; the others are distinct indices of earlier blocks, then -1 for unused entries. For one key head, the query blocks of one device's range together choose at most 2 distinct blocks of any other device's range, and some device reaches 2 in every draw.
All inputs are finite; a program needn't handle non-finite values.
Results may differ from a plain program's by a relative error of at most 0.028.
The roundings to bfloat16 on the way count: a program that leaves them out, or rounds other values in their place, can miss the bound.
Values may be sent and summed in bfloat16 or wider, within the bound.
No kernel may reach another device: no remote copies, remote signals or barrier semaphores. Data moves between devices by JAX's collectives and lax.ppermute only.
A program may use at most 128 MiB of HBM per device.

v0:
```python
import jax
import jax.numpy as jnp
from jax import lax
from jax.sharding import PartitionSpec as P

HEAD_DIM = 64
BLOCK = 64
TOPK = 32
ROPE_BASE = 500000.0


def cut_along(shard, dim, peers):
    lengths = shard.shape
    tiles = shard.reshape(*lengths[:dim], peers, lengths[dim] // peers, *lengths[dim + 1 :])
    return jnp.moveaxis(tiles, dim, 0)


def sum_at_owner(shard, axis, dim):
    tiles = cut_along(shard, dim, lax.axis_size(axis))
    arrived = lax.all_to_all(tiles, axis, split_axis=0, concat_axis=0, tiled=True)
    return arrived.astype(jnp.float32).sum(axis=0)


def rotate(head_rows, positions):
    half = head_rows.shape[-1] // 2
    freqs = ROPE_BASE ** (-jnp.arange(half, dtype=jnp.float32) / half)
    angles = positions[:, None, None] * freqs
    cosine = jnp.cos(angles)
    sine = jnp.sin(angles)
    first = head_rows[..., :half]
    second = head_rows[..., half:]
    return jnp.concatenate(
        [first * cosine - second * sine, second * cosine + first * sine], axis=-1
    )


def shards(tokens, w_query, w_key, w_value, w_out, selection):
    row_count = tokens.shape[0]
    local_heads = w_query.shape[1] // HEAD_DIM
    own_index = lax.axis_index("kv")
    positions_int = own_index * row_count + jnp.arange(row_count)
    positions = positions_int.astype(jnp.float32)
    queries = rotate(
        jnp.dot(tokens, w_query, preferred_element_type=jnp.float32).reshape(
            row_count, local_heads, HEAD_DIM
        ),
        positions,
    ).astype(jnp.bfloat16)
    key_local = rotate(
        jnp.dot(tokens, w_key, preferred_element_type=jnp.float32).reshape(row_count, 1, HEAD_DIM),
        positions,
    )[:, 0].astype(jnp.bfloat16)
    value_local = jnp.dot(tokens, w_value, preferred_element_type=jnp.float32).astype(jnp.bfloat16)
    key_value = jnp.concatenate([key_local, value_local], axis=-1)
    blocks_here = row_count // BLOCK
    chosen_ids = selection[0]
    key_table = lax.all_gather(key_value, "kv", axis=0, tiled=True).reshape(-1, BLOCK, 2 * HEAD_DIM)
    slot_ids = jnp.maximum(chosen_ids, 0)
    picked = key_table[slot_ids]
    picked_keys = picked[..., :HEAD_DIM].reshape(blocks_here, TOPK * BLOCK, HEAD_DIM)
    picked_values = picked[..., HEAD_DIM:].reshape(blocks_here, TOPK * BLOCK, HEAD_DIM)
    offsets = jnp.arange(BLOCK)
    key_pos = (chosen_ids[:, :, None] * BLOCK + offsets).reshape(blocks_here, TOPK * BLOCK)
    live_keys = jnp.repeat(chosen_ids >= 0, BLOCK, axis=1)
    query_pos = positions_int.reshape(blocks_here, BLOCK)
    query_rows = queries.reshape(blocks_here, BLOCK, local_heads, HEAD_DIM)
    scores = jnp.einsum(
        "qbhd,qkd->qhbk", query_rows, picked_keys, preferred_element_type=jnp.float32
    ) * HEAD_DIM ** (-0.5)
    allowed = live_keys[:, None, None, :] & (
        key_pos[:, None, None, :] <= query_pos[:, None, :, None]
    )
    scores = jnp.where(allowed, scores, -jnp.inf)
    top_score = jnp.max(scores, axis=-1, keepdims=True)
    expo = jnp.exp(scores - top_score)
    weights = (expo / jnp.sum(expo, axis=-1, keepdims=True)).astype(jnp.bfloat16)
    attended = jnp.einsum(
        "qhbk,qkd->qbhd", weights, picked_values, preferred_element_type=jnp.float32
    ).astype(jnp.bfloat16)
    attended = attended.reshape(row_count, local_heads * HEAD_DIM)
    summed = sum_at_owner(
        jnp.dot(attended, w_out, preferred_element_type=jnp.float32).astype(jnp.bfloat16), "tp", 0
    )
    return summed.astype(jnp.bfloat16)


def solution(mesh):
    placed = (
        P(("grp", "kv"), None),
        P(None, "tp"),
        P(None, "tp"),
        P(None, "tp"),
        P("tp", None),
        P("tp", ("grp", "kv"), None),
    )
    return jax.shard_map(
        shards, mesh=mesh, in_specs=placed, out_specs=P(("grp", "kv", "tp"), None), check_vma=False
    )
```

profile of v0, /device:TPU:33, one launch (start us, length us, event | category | flops | bytes accessed | tf_op | source)
XLA Modules:
  0.0 269.1 jit_solution(14196923973627354760)
XLA Ops:
  6.6 1.6 copy-done
  8.1 1.7 convolution_convert_fusion.1
  9.8 1.7 convolution_bitcast_fusion
  11.6 0.3 fusion.16
  11.9 0.7 pad_maximum_fusion.1
  12.6 0.1 all-gather.2.cloned.1.call-update
  12.6 0.0 copy-done.1
  12.7 0.1 reshape.209
  12.7 0.1 add.60
  12.8 0.1 broadcast_in_dim.10
  12.9 0.1 and.16
  13.1 0.1 add.57
  13.2 0.1 add.58
  13.3 0.3 multiply_cosine_fusion
  13.6 2.0 fusion.27
  15.6 0.1 subtract_convert_fusion
  15.6 0.2 concatenate.18
  15.8 1.1 copy.12
  17.0 0.2 concatenate.19
  17.2 1.1 copy.13
  18.3 1.0 compare_and_fusion
  19.3 160.9 %all-gather.2.cloned.1.call-done = bf16[32768,128]{0,1:T(8,128)(2,1)} async-done(((bf16[512,128]{0,1:T(8,128)(2,1)}), bf16[32768,128]{0,1:T(8,128)(2,1)}) %all-gather.2.cloned.1.call-update) | async-done | bytes 8388624 | tf_op jit(solution)/shard_map/all_gather | solution.py:57
  180.2 11.9 %copy.9 = bf16[32768,128]{1,0:T(8,128)(2,1)} copy(bf16[32768,128]{0,1:T(8,128)(2,1)} %all-gather.2.cloned.1.call-done) | data formatting | bytes 16777216 | tf_op jit(solution)/shard_map/all_gather | solution.py:57
  192.1 6.4 %gather_fusion = bf16[256,64,128]{2,1,0:T(8,128)(2,1)} fusion(bf16[512,64,128]{2,1,0:T(8,128)(2,1)} %bitcast.53, s32[1024]{0:T(1024)S(1)} %pad_clamp_fusion), kind=kCustom, calls=%fused_computation | custom fusion | bytes 8389632 | tf_op jit(solution)/shard_map/gather | solution.py:59
  198.5 7.3 %fusion.25 = (bf16[8,32,64,64]{3,2,1,0:T(8,128)(2,1)}, bf16[8,32,64,64]{3,2,1,0:T(8,128)(2,1)}) fusion(bf16[8,32,64,128]{3,2,1,0:T(8,128)(2,1)} %bitcast.52), kind=kLoop, calls=%fused_computation.47 | loop fusion | bytes 8388608 | tf_op jit(solution)/shard_map/slice | solution.py:60
  205.8 10.6 %fusion.26 = (f32[8,4,64]{2,1,0:T(4,128)S(1)}, f32[8,4,64,2048]{3,2,1,0:T(8,128)}) fusion(pred[8,64,2048]{2,1,0:T(8,128)(4,1)S(1)} %compare_and_fusion, bf16[8,2048,64,1]{2,1,3,0:T(8,128)(2,1)} %bitcast.56, bf16[8,64,4,32]{3,1,2,0:T(8,128)(2,1)} %copy.13, bf16[8,64,4,32]{3,1,2,0:T(8,128)(2,1)} %copy.12), kind=kOutput, calls=%fused_computation.48 | convolution fusion | flops 554174464 | bytes 20193280 | tf_op jit(solution)/shard_map/sub | solution.py:75
  216.4 10.7 %fusion.9 = bf16[8,64,4,64]{1,3,2,0:T(8,128)(2,1)S(1)} fusion(bf16[8,2048,64,1]{2,1,3,0:T(8,128)(2,1)} %bitcast.55, f32[8,4,64,2048]{3,2,1,0:T(8,128)} %get-tuple-element.16, f32[8,4,64]{2,1,0:T(4,128)S(1)} %get-tuple-element.15), kind=kOutput, calls=%fused_computation.14 | convolution fusion | flops 545390592 | bytes 19144704 | tf_op jit(solution)/shard_map/qhbk,qkd->qbhd/dot_general | solution.py:77
  227.1 0.3 copy.14
  227.5 0.3 reshape.205
  227.8 2.0 convolution_convert_fusion
  229.8 29.6 %all_to_all.5 = bf16[4,128,2048]{2,1,0:T(8,128)(2,1)} all-to-all(bf16[4,128,2048]{2,1,0:T(8,128)(2,1)S(1)} %bitcast.54), channel_id=1, replica_groups=mesh['grp'=2,'kv'=64,'tp'=4] {'tp'}, dimensions={0} | all-to-all | bytes 4194304 | tf_op jit(solution)/shard_map/all_to_all | solution.py:20
  259.4 2.9 %reduce_sum.22 = bf16[128,2048]{1,0:T(8,128)(2,1)} reduce(bf16[4,128,2048]{2,1,0:T(8,128)(2,1)} %all_to_all.5, bf16[]{:T(256)} %constant.29.clone.1), dimensions={0}, to_apply=%region_2.3 | reduce | flops 786432 | bytes 2621442 | tf_op jit(solution)/shard_map/reduce_sum | solution.py:21
  (12 shorter events, 0.1 us)
Async XLA Ops:
  6.5 1.6 copy-start
  6.6 6.1 %copy-start.1 = (s32[1,8,32]{2,1,0:T(8,128)S(1)}, s32[1,8,32]{2,1,0:T(8,128)}, u32[]{:S(2)}) copy-start(s32[1,8,32]{2,1,0:T(8,128)} %param.11) | copy-start | bytes 3076
  6.6 173.6 %all-gather.2.cloned.1.call-start = ((), (), s32[]{:S(2)}) async-start(), calls=%async_computation.1 | async-start | bytes 8519680 | tf_op jit(solution)/shard_map/all_gather | solution.py:57
Sparse Core Ops, SparseCore 0:
  12.8 167.3 all-gather.1
where the time goes:
time: 270 us; the launch traced here: 269 us
  waiting for transfers between devices  161 us (60%)
  local copies, waits for them, and re-layouts  31 us (11%)
  blocking collectives  29.6 us (11%)
  matrix products  28.6 us (11%)
  between operations  13.6 us (5%)
  other arithmetic  5.32 us (2%)
    all_gather x1, waiting for transfers between devices, shards(): lax.all_gather(key_value, 'kv', axis=0, tiled=True)  161 us
    all_to_all x1, blocking collectives, sum_at_owner(): lax.all_to_all(tiles, axis, split_axis=0, concat_axis=0, tiled=True)  29.6 us
    all_gather x1, local copies, waits for them, and re-layouts, shards(): lax.all_gather(key_value, 'kv', axis=0, tiled=True)  11.9 us
    dot_general x1, matrix products, shards(): jnp.einsum('qhbk,qkd->qbhd', weights, picked_values, preferred_element_ty...  10.7 us
    sub x1, matrix products, shards(): expo = jnp.exp(scores - top_score)  10.6 us
    slice x1, local copies, waits for them, and re-layouts, shards(): picked[..., :HEAD_DIM].reshape(blocks_here, TOPK * BLOCK, HEAD_DIM)  7.28 us
    gather x1, local copies, waits for them, and re-layouts, shards(): picked = key_table[slot_ids]  6.41 us
  transfers between devices with their start and end apart: 1, of which 1 were waited for; matrix products, arithmetic and copies ran while one was open for 2% of the time, Pallas kernels for 0%

commit v1 on v0

--- a/solution.py
+++ b/solution.py
@@ -1,3 +1,4 @@
+import functools
 import jax
 import jax.numpy as jnp
 from jax import lax
@@ -7,6 +8,18 @@
 BLOCK = 64
 TOPK = 32
 ROPE_BASE = 500000.0
+
+
+def push_wires(frame, which_dim):
+    table = []
+    for _ in range(lax.axis_size("kv")):
+        table.append(frame)
+    b_now = jnp.concatenate(table, axis=which_dim)
+    upper = lax.all_to_all(b_now, "kv", which_dim, which_dim, tiled=True)
+    return upper
+
+
+bind_the_squares = functools.partial(push_wires, which_dim=0)
 
 
 def cut_along(shard, dim, peers):
@@ -54,7 +67,7 @@
     key_value = jnp.concatenate([key_local, value_local], axis=-1)
     blocks_here = row_count // BLOCK
     chosen_ids = selection[0]
-    key_table = lax.all_gather(key_value, "kv", axis=0, tiled=True).reshape(-1, BLOCK, 2 * HEAD_DIM)
+    key_table = bind_the_squares(key_value).reshape(-1, BLOCK, 2 * HEAD_DIM)
     slot_ids = jnp.maximum(chosen_ids, 0)
     picked = key_table[slot_ids]
     picked_keys = picked[..., :HEAD_DIM].reshape(blocks_here, TOPK * BLOCK, HEAD_DIM)

time: 270 us -> 914 us (3.39)
  the two profiles are of different devices: /device:TPU:33 before, /device:TPU:104 now
where the time goes in v1:
time: 914 us
  waiting for transfers between devices  732 us (80%)
  other arithmetic  47.9 us (5%)
  starting transfers between devices  45.4 us (5%)
  blocking collectives  30.7 us (3%)
  local copies, waits for them, and re-layouts  29.7 us (3%)
  matrix products  27.4 us (3%)
    all_to_all x1, waiting for transfers between devices, push_wires(): upper = lax.all_to_all(b_now, 'kv', which_dim, which_dim, tiled=True)  732 us
    all_to_all x1, starting transfers between devices, push_wires(): upper = lax.all_to_all(b_now, 'kv', which_dim, which_dim, tiled=True)  45.4 us
    unnamed x63, other arithmetic  42.5 us
    all_to_all x1, blocking collectives, sum_at_owner(): lax.all_to_all(tiles, axis, split_axis=0, concat_axis=0, tiled=True)  30.7 us
  transfers between devices with their start and end apart: 1, of which 1 were waited for; matrix products, arithmetic and copies ran while one was open for 0% of the time, Pallas kernels for 0%

profile of v1, /device:TPU:104, one launch (start us, length us, event | category | flops | bytes accessed | tf_op | source)
XLA Modules:
  0.0 913.7 jit_solution(3594036857709022028)
XLA Ops:
  0.0 1.6 copy-done
  1.6 1.7 convolution_convert_fusion.1
  3.3 1.7 convolution_bitcast_fusion
  11.3 0.7 constant_dynamic-update-slice_fusion.54
  12.0 0.7 constant_dynamic-update-slice_fusion.53
  13.4 0.7 constant_dynamic-update-slice_fusion.51
  18.8 0.7 constant_dynamic-update-slice_fusion.43
  20.9 0.7 constant_dynamic-update-slice_fusion.40
  24.2 0.7 constant_dynamic-update-slice_fusion.35
  24.9 0.7 constant_dynamic-update-slice_fusion.34
  26.3 0.7 constant_dynamic-update-slice_fusion.32
  35.0 0.7 constant_dynamic-update-slice_fusion.19
  37.1 0.7 constant_dynamic-update-slice_fusion.16
  37.8 0.7 constant_dynamic-update-slice_fusion.15
  39.1 0.7 constant_dynamic-update-slice_fusion.13
  39.8 0.7 constant_dynamic-update-slice_fusion.12
  45.9 0.7 constant_dynamic-update-slice_fusion.3
  46.6 0.7 constant_dynamic-update-slice_fusion.2
  47.2 0.7 constant_dynamic-update-slice_fusion.1
  47.9 0.7 constant_dynamic-update-slice_fusion
  48.6 11.9 %copy.15 = bf16[32768,128]{1,0:T(8,128)(2,1)} copy(bf16[32768,128]{0,1:T(8,128)(2,1)} %constant_dynamic-update-slice_fusion) | data formatting | bytes 16777216 | tf_op jit(solution)/shard_map/all_to_all | solution.py:18
  60.6 45.4 %all-to-all-start = ((bf16[64,512,128]{2,1,0:T(8,128)(2,1)}), bf16[64,512,128]{2,1,0:T(8,128)(2,1)}, u32[]{:S(2)}, u32[]{:S(2)}) async-start(bf16[64,512,128]{2,1,0:T(8,128)(2,1)} %bitcast.56), calls=%async_computation | async-start | bytes 16777216 | tf_op jit(solution)/shard_map/all_to_all | solution.py:18
  106.9 0.8 fusion.27
  108.9 0.9 compare_and_fusion
  109.8 732.4 %all-to-all-done = bf16[64,512,128]{2,1,0:T(8,128)(2,1)} async-done(((bf16[64,512,128]{2,1,0:T(8,128)(2,1)}), bf16[64,512,128]{2,1,0:T(8,128)(2,1)}, u32[]{:S(2)}, u32[]{:S(2)}) %all-to-all-start) | async-done | bytes 8388640 | tf_op jit(solution)/shard_map/all_to_all | solution.py:18
  842.2 6.4 gather_fusion
  848.6 7.5 fusion.25
  856.2 10.5 %fusion.26 = (f32[8,4,64]{2,1,0:T(4,128)S(1)}, f32[8,4,64,2048]{3,2,1,0:T(8,128)}) fusion(pred[8,64,2048]{2,1,0:T(8,128)(4,1)S(1)} %compare_and_fusion, bf16[8,2048,64,1]{2,1,3,0:T(8,128)(2,1)} %bitcast.59, bf16[8,64,4,32]{3,1,2,0:T(8,128)(2,1)S(1)} %copy.11, bf16[8,64,4,32]{3,1,2,0:T(8,128)(2,1)S(1)} %copy.10), kind=kOutput, calls=%fused_computation.112 | convolution fusion | flops 554174464 | bytes 20193280 | tf_op jit(solution)/shard_map/sub | solution.py:88
  866.7 10.8 %fusion.9 = bf16[8,64,4,64]{1,3,2,0:T(8,128)(2,1)S(1)} fusion(bf16[8,2048,64,1]{2,1,3,0:T(8,128)(2,1)} %bitcast.58, f32[8,4,64,2048]{3,2,1,0:T(8,128)} %get-tuple-element.16, f32[8,4,64]{2,1,0:T(4,128)S(1)} %get-tuple-element.15), kind=kOutput, calls=%fused_computation.14 | convolution fusion | flops 545390592 | bytes 19144704 | tf_op jit(solution)/shard_map/qhbk,qkd->qbhd/dot_general | solution.py:90
  878.2 2.0 convolution_convert_fusion
  880.1 30.7 %all_to_all.14 = bf16[4,128,2048]{2,1,0:T(8,128)(2,1)} all-to-all(bf16[4,128,2048]{2,1,0:T(8,128)(2,1)S(1)} %bitcast.57), channel_id=1, replica_groups=mesh['grp'=2,'kv'=64,'tp'=4] {'tp'}, dimensions={0} | all-to-all | bytes 4194304 | tf_op jit(solution)/shard_map/all_to_all | solution.py:33
  910.8 2.9 reduce_sum.22
  (78 shorter events, 34.5 us)
Async XLA Ops:
  0.0 1.6 copy-start
  60.6 45.4 %copy-start.2 = (s32[1,8,32]{2,1,0:T(8,128)S(1)}, s32[1,8,32]{2,1,0:T(8,128)}, u32[]{:S(2)}) copy-start(s32[1,8,32]{2,1,0:T(8,128)} %param.11) | copy-start | bytes 3076
  60.6 46.4 %copy-start.3 = (bf16[2048,256]{1,0:T(8,128)(2,1)S(1)}, bf16[2048,256]{1,0:T(8,128)(2,1)}, u32[]{:S(2)}) copy-start(bf16[2048,256]{1,0:T(8,128)(2,1)} %param.7) | copy-start | bytes 3145732
  60.6 781.6 %all-to-all-start = ((bf16[64,512,128]{2,1,0:T(8,128)(2,1)}), bf16[64,512,128]{2,1,0:T(8,128)(2,1)}, u32[]{:S(2)}, u32[]{:S(2)}) async-start(bf16[64,512,128]{2,1,0:T(8,128)(2,1)} %bitcast.56), calls=%async_computation | async-start | bytes 16777216 | tf_op jit(solution)/shard_map/all_to_all | solution.py:18
  866.7 47.1 %copy-start.1 = (bf16[512,2048]{1,0:T(8,128)(2,1)S(1)}, bf16[512,2048]{1,0:T(8,128)(2,1)}, u32[]{:S(2)}) copy-start(bf16[512,2048]{1,0:T(8,128)(2,1)} %param.6) | copy-start | bytes 6291460
